TPU v7x, 32 devices: a whole 2x2x4 slice. The times are simulated.
32 devices in a mesh: kv: 8 (over z, y), tp: 4 (over x, core).
Axes of the slice: x: 2, y: 2, z: 4, core: 2. Of those that a mesh axis runs over, the one named last changes fastest.
Arguments:
- tokens: bfloat16 [128, 4096], P(None, ('kv', 'tp')), may hold values from -64 to 64
- mix_gain: float32 [4096], P('kv'), may hold values from 0.1 to 1.9
- w_query: bfloat16 [4096, 3072], P('kv', 'tp'), may hold values from -0.09375 to 0.09375
- w_key: bfloat16 [4096, 3072], P('kv', 'tp'), may hold values from -0.09375 to 0.09375
- w_value: bfloat16 [4096, 3072], P('kv', 'tp'), may hold values from -0.09375 to 0.09375
- w_gate: bfloat16 [4096, 3072], P('kv', 'tp'), may hold values from -0.09375 to 0.09375
- w_beta: bfloat16 [4096, 24], P('kv'), may hold values from -0.09375 to 0.09375
- w_decay: bfloat16 [4096, 24], P('kv'), may hold values from -0.09375 to 0.09375
- decay_rate: float32 [24], P('tp'), may hold values from 0.15 to 1.5
- out_gain: float32 [128], replicated, may hold values from 0.1 to 1.9
- state: float32 [128, 24, 128, 128], P('kv', 'tp'), may hold values from -0.6 to 0.6
- w_out: bfloat16 [3072, 4096], P('tp', 'kv'), may hold values from -0.109375 to 0.109375
- mlp_gain: float32 [4096], replicated, may hold values from 0.1 to 1.9
- w_up: bfloat16 [4096, 16384], P(None, ('kv', 'tp')), may hold values from -0.09375 to 0.09375
- w_down: bfloat16 [16384, 4096], P(('kv', 'tp')), may hold values from -0.09375 to 0.09375
Outputs:
- mixed: bfloat16 [128, 4096], P(None, ('kv', 'tp'))
- new_state: float32 [128, 24, 128, 128], P('kv', 'tp')
All inputs are finite; a program needn't handle non-finite values.
Results may differ from a plain program's by a relative error of at most 0.0063.
Values may be sent and summed in bfloat16 or wider, within the bound.
A program may use at most 64 MiB of HBM per device.

v0:
```python
import jax
import jax.numpy as jnp
from jax import lax
from jax.sharding import PartitionSpec as P

D = 4096
EPSILON = 1e-06


def head_norm(values):
    return values * lax.rsqrt(jnp.sum(values * values, axis=-1, keepdims=True) + EPSILON)


def feed_forward(segment, mlp_gain, w_up, w_down):
    segment_f = segment.astype(jnp.float32)
    normed_mlp = (
        segment_f
        * lax.rsqrt(jnp.mean(segment_f * segment_f, axis=1, keepdims=True) + EPSILON)
        * mlp_gain[None, :]
    ).astype(jnp.bfloat16)
    hidden = jnp.square(
        jax.nn.relu(jnp.dot(normed_mlp, w_up, preferred_element_type=jnp.float32))
    ).astype(jnp.bfloat16)
    return jnp.dot(hidden, w_down, preferred_element_type=jnp.float32)


def local(
    tokens,
    mix_gain,
    w_query,
    w_key,
    w_value,
    w_gate,
    w_beta,
    w_decay,
    decay_rate,
    out_gain,
    state,
    w_out,
    mlp_gain,
    w_up,
    w_down,
):
    local_rows = state.shape[0]
    local_heads = decay_rate.shape[0]
    head_size = state.shape[2]
    all_heads = w_beta.shape[1]
    columns = lax.all_gather(tokens, "tp", axis=1, tiled=True)
    columns_f = columns.astype(jnp.float32)
    normed = (columns_f * mix_gain[None, :]).astype(jnp.bfloat16)
    part_query = jnp.dot(normed, w_query, preferred_element_type=jnp.float32)
    part_key = jnp.dot(normed, w_key, preferred_element_type=jnp.float32)
    part_value = jnp.dot(normed, w_value, preferred_element_type=jnp.float32)
    part_gate = jnp.dot(normed, w_gate, preferred_element_type=jnp.float32)
    part_rates = jnp.dot(
        normed, jnp.concatenate([w_beta, w_decay], axis=1), preferred_element_type=jnp.float32
    )
    summed = (
        lax.psum_scatter(part_query, "kv", scatter_dimension=0, tiled=True),
        lax.psum_scatter(part_key, "kv", scatter_dimension=0, tiled=True),
        lax.psum_scatter(part_value, "kv", scatter_dimension=0, tiled=True),
        lax.psum_scatter(part_gate, "kv", scatter_dimension=0, tiled=True),
        lax.psum_scatter(part_rates, "kv", scatter_dimension=0, tiled=True),
        lax.psum_scatter(
            jnp.sum(columns_f * columns_f, axis=1), "kv", scatter_dimension=0, tiled=True
        ),
    )
    own_squares = summed[5]
    row_scale = lax.rsqrt(own_squares / D + EPSILON)[:, None]
    shape_heads = (local_rows, local_heads, head_size)
    query = head_norm(jax.nn.silu((summed[0] * row_scale).reshape(shape_heads))) * head_size ** (
        -0.5
    )
    key = head_norm(jax.nn.silu((summed[1] * row_scale).reshape(shape_heads)))
    value = jax.nn.silu((summed[2] * row_scale).reshape(shape_heads))
    gate_raw = (summed[3] * row_scale).reshape(shape_heads)
    rates = summed[4] * row_scale
    head_start = lax.axis_index("tp") * local_heads
    beta = jax.nn.sigmoid(lax.dynamic_slice_in_dim(rates, head_start, local_heads, 1))
    decay_raw = lax.dynamic_slice_in_dim(rates, all_heads + head_start, local_heads, 1)
    decay = jnp.exp(-decay_rate[None, :] * jax.nn.softplus(decay_raw))
    faded = state * decay[:, :, None, None]
    recalled = jnp.einsum("bhkv,bhk->bhv", faded, key, precision=lax.Precision.HIGHEST)
    change = beta[:, :, None] * (value - recalled)
    new_state = faded + key[:, :, :, None] * change[:, :, None, :]
    readout = jnp.einsum("bhkv,bhk->bhv", new_state, query, precision=lax.Precision.HIGHEST)
    scaled = (
        readout
        * lax.rsqrt(jnp.mean(readout * readout, axis=-1, keepdims=True) + EPSILON)
        * out_gain
    )
    merged = (
        (scaled * jax.nn.silu(gate_raw))
        .reshape(local_rows, local_heads * head_size)
        .astype(jnp.bfloat16)
    )
    partial_out = jnp.dot(
        lax.all_gather(merged, "kv", axis=0, tiled=True), w_out, preferred_element_type=jnp.float32
    )
    branch_sum = lax.psum_scatter(partial_out, "tp", scatter_dimension=1, tiled=True)
    residual = (tokens.astype(jnp.float32) + branch_sum).astype(jnp.bfloat16)
    whole_rows = lax.all_gather(residual, ("kv", "tp"), axis=1, tiled=True)
    partial_mlp = feed_forward(whole_rows, mlp_gain, w_up, w_down)
    branch = lax.psum_scatter(partial_mlp, ("kv", "tp"), scatter_dimension=1, tiled=True)
    mixed = (residual.astype(jnp.float32) + branch).astype(jnp.bfloat16)
    return (mixed, new_state)


def solution(mesh):
    placed = (
        P(None, ("kv", "tp")),
        P("kv"),
        P("kv", "tp"),
        P("kv", "tp"),
        P("kv", "tp"),
        P("kv", "tp"),
        P("kv", None),
        P("kv", None),
        P("tp"),
        P(),
        P("kv", "tp", None, None),
        P("tp", "kv"),
        P(),
        P(None, ("kv", "tp")),
        P(("kv", "tp"), None),
    )
    return jax.shard_map(
        local,
        mesh=mesh,
        in_specs=placed,
        out_specs=(P(None, ("kv", "tp")), P("kv", "tp", None, None)),
        check_vma=False,
    )
```

profile of v0, /device:TPU:0, one launch (start us, length us, event | category | flops | bytes accessed | tf_op | source)
XLA Modules:
  0.0 618.0 jit_solution(8560261450145057802)
XLA Ops:
  7.2 0.0 copy-start
  7.2 0.0 copy-start.11
  7.2 0.0 copy-start.7
  7.2 0.0 copy-start.2
  7.2 0.0 reduce-scatter.8.cloned.1.call-start
  7.3 6.9 %all_gather.9 = bf16[128,512]{1,0:T(8,128)(2,1)S(1)} all-gather(bf16[128,128]{1,0:T(8,128)(2,1)} %param.15), channel_id=1, replica_groups=mesh['kv'=8,'tp'=4] {'tp'}, dimensions={1}, use_global_device_ids=true | all-gather | bytes 163840 | tf_op jit(solution)/shard_map/all_gather | solution.py:48
  14.2 1.6 fusion.31
  15.7 0.0 reduce-scatter.8.cloned.1.call-update
  15.8 0.0 reduce-scatter.10.cloned.1.call-start
  15.8 1.7 fusion.29
  17.5 0.0 reduce-scatter.10.cloned.1.call-update
  17.5 0.0 reduce-scatter.12.cloned.1.call-start
  17.6 2.2 fusion.27
  19.8 0.0 reduce-scatter.12.cloned.1.call-update
  19.8 0.0 reduce-scatter.14.cloned.1.call-start
  19.8 1.7 fusion.25
  21.5 0.0 reduce-scatter.14.cloned.1.call-update
  21.6 0.0 reduce-scatter.16.cloned.1.call-start
  21.6 1.0 fusion.23
  22.7 0.0 reduce-scatter.16.cloned.1.call-update
  22.7 0.0 reduce-scatter.18.cloned.1.call-start
  22.8 0.0 copy-done.10
  22.8 0.6 dynamic-slice
  24.0 0.1 fusion.16
  24.1 22.1 %all-reduce = f32[128]{0:T(128)S(1)} all-reduce(f32[128]{0:T(128)S(1)} %fusion.16), channel_id=3, replica_groups=mesh['kv'=8,'tp'=4] {'kv'}, use_global_device_ids=true, to_apply=%region_2.0.clone | all-reduce | flops 128 | bytes 1024
  46.2 0.1 fusion.42
  46.3 33.7 %reduce-scatter.8.cloned.1.call-done = f32[16,48]{1,0:T(8,128)} async-done(((f32[128,48]{1,0:T(8,128)}), f32[16,48]{1,0:T(8,128)}) %reduce-scatter.8.cloned.1.call-update) | async-done | bytes 3088 | tf_op jit(solution)/shard_map/reduce_scatter | solution.py:63
  80.0 0.8 broadcast_multiply_fusion.5
  80.8 0.1 add_divide_fusion
  80.9 63.6 %reduce-scatter.10.cloned.1.call-done = f32[16,768]{1,0:T(8,128)} async-done(((f32[128,768]{1,0:T(8,128)}), f32[16,768]{1,0:T(8,128)}) %reduce-scatter.10.cloned.1.call-update) | async-done | bytes 49168 | tf_op jit(solution)/shard_map/reduce_scatter | solution.py:60
  144.5 64.5 %reduce-scatter.12.cloned.1.call-done = f32[16,768]{1,0:T(8,128)} async-done(((f32[128,768]{1,0:T(8,128)}), f32[16,768]{1,0:T(8,128)}) %reduce-scatter.12.cloned.1.call-update) | async-done | bytes 49168 | tf_op jit(solution)/shard_map/reduce_scatter | solution.py:61
  209.0 64.3 %reduce-scatter.14.cloned.1.call-done = f32[16,768]{1,0:T(8,128)} async-done(((f32[128,768]{1,0:T(8,128)}), f32[16,768]{1,0:T(8,128)}) %reduce-scatter.14.cloned.1.call-update) | async-done | bytes 49168 | tf_op jit(solution)/shard_map/reduce_scatter | solution.py:59
  273.3 64.9 %reduce-scatter.16.cloned.1.call-done = f32[16,768]{1,0:T(8,128)} async-done(((f32[128,768]{1,0:T(8,128)}), f32[16,768]{1,0:T(8,128)}) %reduce-scatter.16.cloned.1.call-update) | async-done | bytes 49168 | tf_op jit(solution)/shard_map/reduce_scatter | solution.py:62
  338.2 1.0 broadcast_multiply_fusion.1
  339.2 0.1 multiply_reduce_fusion.1
  339.3 0.1 fusion.55
  339.4 0.1 broadcast_multiply_fusion
  339.5 0.1 multiply_reduce_fusion
  339.6 0.1 multiply_bitcast_fusion
  339.7 7.7 %fusion = f32[16,6,1,128]{3,2,1,0:T(1,128)S(1)} fusion(f32[16,6,128,128]{3,2,1,0:T(8,128)} %param.25, f32[16,6]{1,0:T(8,128)S(1)} %get-tuple-element.3, f32[16,6,128,1]{2,1,0,3:T(8,128)S(1)} %fusion.55), kind=kOutput, calls=%fused_computation.1 | convolution fusion | flops 20447232 | bytes 6390144 | tf_op jit(solution)/shard_map/bhkv,bhk->bhv/dot_general | solution.py:83
  347.5 0.1 fusion.22
  347.6 4.5 multiply_add_fusion
  352.1 0.0 copy-start.1
  352.1 2.7 copy-done.1
  354.8 5.4 fusion.36
  360.2 0.1 fusion.18
  360.3 0.1 fusion.21
  360.4 30.7 %all_gather.10 = bf16[128,768]{1,0:T(8,128)(2,1)S(1)} all-gather(bf16[16,768]{1,0:T(8,128)(2,1)S(1)} %bitcast.34), channel_id=1, replica_groups=mesh['kv'=8,'tp'=4] {'kv'}, dimensions={0}, use_global_device_ids=true | all-gather | bytes 221184 | tf_op jit(solution)/shard_map/all_gather | solution.py:98
  391.2 0.0 copy-done.4
  391.2 1.0 fusion.45
  392.1 0.0 reduce-scatter.18.cloned.1.call-update
  392.2 0.0 all-gather.2.cloned.1.call-start
  392.2 19.3 %reduce-scatter.18.cloned.1.call-done = f32[128,128]{1,0:T(8,128)} async-done(((f32[128,512]{1,0:T(8,128)}), f32[128,128]{1,0:T(8,128)}) %reduce-scatter.18.cloned.1.call-update) | async-done | bytes 65552 | tf_op jit(solution)/shard_map/reduce_scatter | solution.py:100
  411.5 1.5 add_convert_fusion.1
  412.9 0.0 all-gather.2.cloned.1.call-update
  413.0 0.0 reduce-scatter.20.cloned.1.call-start
  413.0 50.4 %all-gather.2.cloned.1.call-done = bf16[128,4096]{1,0:T(8,128)(2,1)} async-done(((bf16[128,128]{1,0:T(8,128)(2,1)}), bf16[128,4096]{1,0:T(8,128)(2,1)}) %all-gather.2.cloned.1.call-update) | async-done | bytes 1048592 | tf_op jit(solution)/shard_map/all_gather | solution.py:102
  463.4 1.5 fusion.3
  464.9 0.0 copy-done.8
  464.9 0.0 copy-start.5
  464.9 6.6 %fusion.8 = f32[128,4096]{1,0:T(8,128)} fusion(bf16[512,4096]{1,0:T(8,128)(2,1)} %param.29, bf16[4096,512]{1,0:T(8,128)(2,1)} %param.28, bf16[128,4096]{1,0:T(8,128)(2,1)} %all-gather.2.cloned.1.call-done, f32[4096]{0:T(1024)S(1)} %copy-done.8, f32[128]{0:T(128)S(1)} %add_rsqrt_fusion.3), kind=kOutput, calls=%fused_computation.12 | convolution fusion | flops 1076035584 | bytes 11551232 | tf_op jit(solution)/shard_map/dot_general | solution.py:24
  471.5 0.0 reduce-scatter.20.cloned.1.call-update
  471.5 138.2 %reduce-scatter.20.cloned.1.call-done = f32[128,128]{1,0:T(8,128)} async-done(((f32[128,4096]{1,0:T(8,128)}), f32[128,128]{1,0:T(8,128)}) %reduce-scatter.20.cloned.1.call-update) | async-done | bytes 65552 | tf_op jit(solution)/shard_map/reduce_scatter | solution.py:104
  609.7 1.5 add_convert_fusion
  (24 shorter events, 0.1 us)
Async XLA Ops:
  7.2 8.6 %copy-start = (bf16[512,768]{1,0:T(8,128)(2,1)S(1)}, bf16[512,768]{1,0:T(8,128)(2,1)}, u32[]{:S(2)}) copy-start(bf16[512,768]{1,0:T(8,128)(2,1)} %param.18) | copy-start | bytes 2359300
  7.2 15.6 %copy-start.11 = (u32[32]{0:T(128)S(1)}, u32[32]{0:T(128)}, u32[]{:S(2)}) copy-start(u32[32]{0:T(128)} %constant.45) | copy-start | bytes 388
  7.2 14.4 %copy-start.7 = (f32[512]{0:T(512)S(1)}, f32[512]{0:T(512)}, u32[]{:S(2)}) copy-start(f32[512]{0:T(512)} %param.16) | copy-start | bytes 6148
  7.2 12.6 %copy-start.2 = (bf16[512,768]{1,0:T(8,128)(2,1)S(1)}, bf16[512,768]{1,0:T(8,128)(2,1)}, u32[]{:S(2)}) copy-start(bf16[512,768]{1,0:T(8,128)(2,1)} %param.17) | copy-start | bytes 2359300
  7.2 14.4 %copy-start.3 = (bf16[512,768]{1,0:T(8,128)(2,1)S(1)}, bf16[512,768]{1,0:T(8,128)(2,1)}, u32[]{:S(2)}) copy-start(bf16[512,768]{1,0:T(8,128)(2,1)} %param.20) | copy-start | bytes 2359300
  7.2 15.5 %copy-start.10 = (f32[6]{0:T(128)S(1)}, f32[6]{0:T(128)}, u32[]{:S(2)}) copy-start(f32[6]{0:T(128)} %param.23) | copy-start | bytes 76
  7.2 72.8 %reduce-scatter.8.cloned.1.call-start = ((), (), s32[]{:S(2)}) async-start(), calls=%async_computation.7 | async-start | bytes 73728 | tf_op jit(solution)/shard_map/reduce_scatter | solution.py:63
  15.8 128.7 %reduce-scatter.10.cloned.1.call-start = ((), (), s32[]{:S(2)}) async-start(), calls=%async_computation.8 | async-start | bytes 442368 | tf_op jit(solution)/shard_map/reduce_scatter | solution.py:60
  17.5 191.4 %reduce-scatter.12.cloned.1.call-start = ((), (), s32[]{:S(2)}) async-start(), calls=%async_computation.9 | async-start | bytes 442368 | tf_op jit(solution)/shard_map/reduce_scatter | solution.py:61
  19.8 253.5 %reduce-scatter.14.cloned.1.call-start = ((), (), s32[]{:S(2)}) async-start(), calls=%async_computation.10 | async-start | bytes 442368 | tf_op jit(solution)/shard_map/reduce_scatter | solution.py:59
  21.6 316.6 %reduce-scatter.16.cloned.1.call-start = ((), (), s32[]{:S(2)}) async-start(), calls=%async_computation.11 | async-start | bytes 442368 | tf_op jit(solution)/shard_map/reduce_scatter | solution.py:62
  22.7 388.8 %reduce-scatter.18.cloned.1.call-start = ((), (), s32[]{:S(2)}) async-start(), calls=%async_computation.12 | async-start | bytes 327680 | tf_op jit(solution)/shard_map/reduce_scatter | solution.py:100
  352.1 2.7 copy-start.1
  354.8 5.6 copy-start.9
  354.8 36.4 %copy-start.4 = (bf16[768,512]{1,0:T(8,128)(2,1)S(1)}, bf16[768,512]{1,0:T(8,128)(2,1)}, u32[]{:S(2)}) copy-start(bf16[768,512]{1,0:T(8,128)(2,1)} %param.26) | copy-start | bytes 2359300
  354.8 56.7 %copy-start.6 = (bf16[128,128]{1,0:T(8,128)(2,1)S(1)}, bf16[128,128]{1,0:T(8,128)(2,1)}, u32[]{:S(2)}) copy-start(bf16[128,128]{1,0:T(8,128)(2,1)} %param.15) | copy-start | bytes 98308
  354.8 110.1 %copy-start.8 = (f32[4096]{0:T(1024)S(1)}, f32[4096]{0:T(1024)}, u32[]{:S(2)}) copy-start(f32[4096]{0:T(1024)} %param.27) | copy-start | bytes 49156
  392.2 71.2 %all-gather.2.cloned.1.call-start = ((), (), s32[]{:S(2)}) async-start(), calls=%async_computation.13 | async-start | bytes 1081344 | tf_op jit(solution)/shard_map/all_gather | solution.py:102
  413.0 196.7 %reduce-scatter.20.cloned.1.call-start = ((), (), s32[]{:S(2)}) async-start(), calls=%async_computation.14 | async-start | bytes 2162688 | tf_op jit(solution)/shard_map/reduce_scatter | solution.py:104
  464.9 144.8 %copy-start.5 = (bf16[128,128]{1,0:T(8,128)(2,1)S(1)}, bf16[128,128]{1,0:T(8,128)(2,1)}, u32[]{:S(2)}) copy-start(bf16[128,128]{1,0:T(8,128)(2,1)} %add_convert_fusion.1) | copy-start | bytes 98308
Sparse Core Ops, SparseCore 0:
  15.9 64.0 reduce-scatter.7
  83.3 61.1 reduce-scatter.9
  147.8 61.1 reduce-scatter.11
  212.1 61.1 reduce-scatter.13
  277.0 61.1 reduce-scatter.15
  392.3 19.1 reduce-scatter.17
  414.9 48.4 all-gather.1
  471.6 138.0 reduce-scatter.19
where the time goes:
time: 619 us; the launch traced here: 618 us
  waiting for transfers between devices  499 us (81%)
  blocking collectives  59.7 us (10%)
  matrix products  28.8 us (5%)
  between operations  15.1 us (2%)
  other arithmetic  11.7 us (2%)
    reduce_scatter x1, waiting for transfers between devices, local(): lax.psum_scatter(partial_mlp, ('kv', 'tp'), scatter_dimension=1, tiled=True)  138 us
    reduce_scatter x1, waiting for transfers between devices, local(): lax.psum_scatter(part_gate, 'kv', scatter_dimension=0, tiled=True)  64.9 us
    reduce_scatter x1, waiting for transfers between devices, local(): lax.psum_scatter(part_value, 'kv', scatter_dimension=0, tiled=True)  64.5 us
    reduce_scatter x1, waiting for transfers between devices, local(): lax.psum_scatter(part_query, 'kv', scatter_dimension=0, tiled=True)  64.3 us
    reduce_scatter x1, waiting for transfers between devices, local(): lax.psum_scatter(part_key, 'kv', scatter_dimension=0, tiled=True)  63.6 us
    all_gather x1, waiting for transfers between devices, local(): whole_rows = lax.all_gather(residual, ('kv', 'tp'), axis=1, tiled=True)  50.4 us
    reduce_scatter x1, waiting for transfers between devices, local(): lax.psum_scatter(part_rates, 'kv', scatter_dimension=0, tiled=True)  33.7 us
    all_gather x1, blocking collectives, local(): lax.all_gather(merged, 'kv', axis=0, tiled=True)  30.7 us
  transfers between devices with their start and end apart: 8, of which 8 were waited for; matrix products, arithmetic and copies ran while one was open for 1% of the time, Pallas kernels for 0%

commit v1 on v0

--- a/solution.py
+++ b/solution.py
@@ -99,7 +99,8 @@
     )
     branch_sum = lax.psum_scatter(partial_out, "tp", scatter_dimension=1, tiled=True)
     residual = (tokens.astype(jnp.float32) + branch_sum).astype(jnp.bfloat16)
-    whole_rows = lax.all_gather(residual, ("kv", "tp"), axis=1, tiled=True)
+    blocks = lax.all_gather(residual, ("kv", "tp"), axis=0, tiled=False)
+    whole_rows = jnp.concatenate(blocks, axis=1)
     partial_mlp = feed_forward(whole_rows, mlp_gain, w_up, w_down)
     branch = lax.psum_scatter(partial_mlp, ("kv", "tp"), scatter_dimension=1, tiled=True)
     mixed = (residual.astype(jnp.float32) + branch).astype(jnp.bfloat16)

time: 619 us -> 630 us (1.018)
  no operation moved by 1% of the time
where the time goes in v1:
time: 630 us; the launch traced here: 629 us
  waiting for transfers between devices  503 us (80%)
  blocking collectives  59.7 us (9%)
  matrix products  28.8 us (5%)
  other arithmetic  16.2 us (3%)
  between operations  15.1 us (2%)
    reduce_scatter x1, waiting for transfers between devices, local(): lax.psum_scatter(partial_mlp, ('kv', 'tp'), scatter_dimension=1, tiled=True)  138 us
    reduce_scatter x1, waiting for transfers between devices, local(): lax.psum_scatter(part_gate, 'kv', scatter_dimension=0, tiled=True)  64.9 us
    reduce_scatter x1, waiting for transfers between devices, local(): lax.psum_scatter(part_value, 'kv', scatter_dimension=0, tiled=True)  64.5 us
    reduce_scatter x1, waiting for transfers between devices, local(): lax.psum_scatter(part_query, 'kv', scatter_dimension=0, tiled=True)  64.3 us
    reduce_scatter x1, waiting for transfers between devices, local(): lax.psum_scatter(part_key, 'kv', scatter_dimension=0, tiled=True)  63.6 us
    all_gather x1, waiting for transfers between devices, local(): blocks = lax.all_gather(residual, ('kv', 'tp'), axis=0, tiled=False)  55.4 us
    reduce_scatter x1, waiting for transfers between devices, local(): lax.psum_scatter(part_rates, 'kv', scatter_dimension=0, tiled=True)  33.7 us
    all_gather x1, blocking collectives, local(): lax.all_gather(merged, 'kv', axis=0, tiled=True)  30.7 us
  transfers between devices with their start and end apart: 8, of which 8 were waited for; matrix products, arithmetic and copies ran while one was open for 1% of the time, Pallas kernels for 0%

profile of v1, /device:TPU:0, one launch (start us, length us, event | category | flops | bytes accessed | tf_op | source)
XLA Modules:
  0.0 629.0 jit_solution(8624223406759319436)
XLA Ops:
  7.2 0.0 copy-start
  7.2 0.0 copy-start.11
  7.2 0.0 copy-start.7
  7.2 0.0 reduce-scatter.8.cloned.1.call-start
  7.3 6.9 %all_gather.12 = bf16[128,512]{1,0:T(8,128)(2,1)S(1)} all-gather(bf16[128,128]{1,0:T(8,128)(2,1)} %param.15), channel_id=1, replica_groups=mesh['kv'=8,'tp'=4] {'tp'}, dimensions={1}, use_global_device_ids=true | all-gather | bytes 163840 | tf_op jit(solution)/shard_map/all_gather | solution.py:48
  14.2 1.6 fusion.24
  15.7 0.0 reduce-scatter.8.cloned.1.call-update
  15.8 0.0 reduce-scatter.10.cloned.1.call-start
  15.8 1.7 fusion.22
  17.5 0.0 reduce-scatter.10.cloned.1.call-update
  17.5 0.0 reduce-scatter.12.cloned.1.call-start
  17.6 2.2 fusion.20
  19.8 0.0 reduce-scatter.12.cloned.1.call-update
  19.8 0.0 reduce-scatter.14.cloned.1.call-start
  19.8 1.7 fusion.18
  21.5 0.0 reduce-scatter.14.cloned.1.call-update
  21.6 0.0 reduce-scatter.16.cloned.1.call-start
  21.6 0.0 copy-done.7
  21.6 0.0 copy-done.3
  21.6 1.0 fusion.16
  22.7 0.0 reduce-scatter.16.cloned.1.call-update
  22.7 0.0 reduce-scatter.18.cloned.1.call-start
  22.8 0.6 dynamic-slice
  24.0 0.1 fusion.9
  24.1 22.1 %all-reduce = f32[128]{0:T(128)S(1)} all-reduce(f32[128]{0:T(128)S(1)} %fusion.9), channel_id=4, replica_groups=mesh['kv'=8,'tp'=4] {'kv'}, use_global_device_ids=true, to_apply=%region_2.0.clone | all-reduce | flops 128 | bytes 1024
  46.2 0.1 fusion.35
  46.3 33.7 %reduce-scatter.8.cloned.1.call-done = f32[16,48]{1,0:T(8,128)} async-done(((f32[128,48]{1,0:T(8,128)}), f32[16,48]{1,0:T(8,128)}) %reduce-scatter.8.cloned.1.call-update) | async-done | bytes 3088 | tf_op jit(solution)/shard_map/reduce_scatter | solution.py:63
  80.0 0.8 broadcast_multiply_fusion.5
  80.7 0.1 add_divide_fusion
  80.8 63.6 %reduce-scatter.10.cloned.1.call-done = f32[16,768]{1,0:T(8,128)} async-done(((f32[128,768]{1,0:T(8,128)}), f32[16,768]{1,0:T(8,128)}) %reduce-scatter.10.cloned.1.call-update) | async-done | bytes 49168 | tf_op jit(solution)/shard_map/reduce_scatter | solution.py:60
  144.4 64.5 %reduce-scatter.12.cloned.1.call-done = f32[16,768]{1,0:T(8,128)} async-done(((f32[128,768]{1,0:T(8,128)}), f32[16,768]{1,0:T(8,128)}) %reduce-scatter.12.cloned.1.call-update) | async-done | bytes 49168 | tf_op jit(solution)/shard_map/reduce_scatter | solution.py:61
  208.9 64.3 %reduce-scatter.14.cloned.1.call-done = f32[16,768]{1,0:T(8,128)} async-done(((f32[128,768]{1,0:T(8,128)}), f32[16,768]{1,0:T(8,128)}) %reduce-scatter.14.cloned.1.call-update) | async-done | bytes 49168 | tf_op jit(solution)/shard_map/reduce_scatter | solution.py:59
  273.3 64.9 %reduce-scatter.16.cloned.1.call-done = f32[16,768]{1,0:T(8,128)} async-done(((f32[128,768]{1,0:T(8,128)}), f32[16,768]{1,0:T(8,128)}) %reduce-scatter.16.cloned.1.call-update) | async-done | bytes 49168 | tf_op jit(solution)/shard_map/reduce_scatter | solution.py:62
  338.2 1.0 broadcast_multiply_fusion.1
  339.2 0.1 multiply_reduce_fusion.2
  339.3 0.1 fusion.49
  339.4 0.1 broadcast_multiply_fusion
  339.5 0.1 multiply_reduce_fusion.1
  339.6 0.1 multiply_bitcast_fusion
  339.7 7.7 %fusion = f32[16,6,1,128]{3,2,1,0:T(1,128)S(1)} fusion(f32[16,6,128,128]{3,2,1,0:T(8,128)} %param.25, f32[16,6]{1,0:T(8,128)S(1)} %get-tuple-element.3, f32[16,6,128,1]{2,1,0,3:T(8,128)S(1)} %fusion.49), kind=kOutput, calls=%fused_computation.1 | convolution fusion | flops 20447232 | bytes 6390144 | tf_op jit(solution)/shard_map/bhkv,bhk->bhv/dot_general | solution.py:83
  347.5 0.1 fusion.15
  347.6 4.5 multiply_add_fusion
  352.1 0.0 copy-start.1
  352.1 2.7 copy-done.1
  354.8 5.4 fusion.29
  360.2 0.1 fusion.11
  360.3 0.1 fusion.14
  360.4 30.7 %all_gather.13 = bf16[128,768]{1,0:T(8,128)(2,1)S(1)} all-gather(bf16[16,768]{1,0:T(8,128)(2,1)S(1)} %bitcast.47), channel_id=1, replica_groups=mesh['kv'=8,'tp'=4] {'kv'}, dimensions={0}, use_global_device_ids=true | all-gather | bytes 221184 | tf_op jit(solution)/shard_map/all_gather | solution.py:98
  391.1 1.0 fusion.38
  392.1 0.0 reduce-scatter.18.cloned.1.call-update
  392.1 0.0 all-gather.3.cloned.1.call-start
  392.2 19.2 %reduce-scatter.18.cloned.1.call-done = f32[128,128]{1,0:T(8,128)} async-done(((f32[128,512]{1,0:T(8,128)}), f32[128,128]{1,0:T(8,128)}) %reduce-scatter.18.cloned.1.call-update) | async-done | bytes 65552 | tf_op jit(solution)/shard_map/reduce_scatter | solution.py:100
  411.4 1.5 add_convert_fusion.1
  412.9 0.0 all-gather.3.cloned.1.call-update
  412.9 0.2 reduce-scatter.20.cloned.1.call-start
  413.1 55.4 %all-gather.3.cloned.1.call-done = bf16[4096,128]{1,0:T(8,128)(2,1)} async-done(((bf16[128,128]{1,0:T(8,128)(2,1)}), bf16[4096,128]{1,0:T(8,128)(2,1)}) %all-gather.3.cloned.1.call-update) | async-done | bytes 1048592 | tf_op jit(solution)/shard_map/all_gather | solution.py:102
  468.5 1.5 multiply_reduce_fusion
  470.1 2.8 bitcast_convert_fusion
  472.9 1.9 copy.18
  474.8 1.7 fusion.4
  476.5 6.5 %fusion.7 = f32[128,4096]{1,0:T(8,128)} fusion(bf16[512,4096]{1,0:T(8,128)(2,1)} %param.29, bf16[128,4096]{0,1:T(8,128)(2,1)} %fusion.4, bf16[4096,512]{1,0:T(8,128)(2,1)} %param.28), kind=kOutput, calls=%fused_computation.11 | convolution fusion | flops 1073938432 | bytes 11534336 | tf_op jit(solution)/shard_map/dot_general | solution.py:24
  483.0 0.0 reduce-scatter.20.cloned.1.call-update
  483.0 137.6 %reduce-scatter.20.cloned.1.call-done = f32[128,128]{1,0:T(8,128)} async-done(((f32[128,4096]{1,0:T(8,128)}), f32[128,128]{1,0:T(8,128)}) %reduce-scatter.20.cloned.1.call-update) | async-done | bytes 65552 | tf_op jit(solution)/shard_map/reduce_scatter | solution.py:105
  620.6 1.5 add_convert_fusion
  (27 shorter events, 0.1 us)
Async XLA Ops:
  7.2 8.6 %copy-start = (bf16[512,768]{1,0:T(8,128)(2,1)S(1)}, bf16[512,768]{1,0:T(8,128)(2,1)}, u32[]{:S(2)}) copy-start(bf16[512,768]{1,0:T(8,128)(2,1)} %param.18) | copy-start | bytes 2359300
  7.2 15.6 %copy-start.11 = (u32[32]{0:T(128)S(1)}, u32[32]{0:T(128)}, u32[]{:S(2)}) copy-start(u32[32]{0:T(128)} %constant.45) | copy-start | bytes 388
  7.2 14.4 %copy-start.7 = (f32[512]{0:T(512)S(1)}, f32[512]{0:T(512)}, u32[]{:S(2)}) copy-start(f32[512]{0:T(512)} %param.16) | copy-start | bytes 6148
  7.2 12.6 %copy-start.2 = (bf16[512,768]{1,0:T(8,128)(2,1)S(1)}, bf16[512,768]{1,0:T(8,128)(2,1)}, u32[]{:S(2)}) copy-start(bf16[512,768]{1,0:T(8,128)(2,1)} %param.17) | copy-start | bytes 2359300
  7.2 14.4 %copy-start.3 = (bf16[512,768]{1,0:T(8,128)(2,1)S(1)}, bf16[512,768]{1,0:T(8,128)(2,1)}, u32[]{:S(2)}) copy-start(bf16[512,768]{1,0:T(8,128)(2,1)} %param.20) | copy-start | bytes 2359300
  7.2 15.5 %copy-start.10 = (f32[6]{0:T(128)S(1)}, f32[6]{0:T(128)}, u32[]{:S(2)}) copy-start(f32[6]{0:T(128)} %param.23) | copy-start | bytes 76
  7.2 72.7 %reduce-scatter.8.cloned.1.call-start = ((), (), s32[]{:S(2)}) async-start(), calls=%async_computation.7 | async-start | bytes 73728 | tf_op jit(solution)/shard_map/reduce_scatter | solution.py:63
  15.8 128.7 %reduce-scatter.10.cloned.1.call-start = ((), (), s32[]{:S(2)}) async-start(), calls=%async_computation.8 | async-start | bytes 442368 | tf_op jit(solution)/shard_map/reduce_scatter | solution.py:60
  17.5 191.4 %reduce-scatter.12.cloned.1.call-start = ((), (), s32[]{:S(2)}) async-start(), calls=%async_computation.9 | async-start | bytes 442368 | tf_op jit(solution)/shard_map/reduce_scatter | solution.py:61
  19.8 253.5 %reduce-scatter.14.cloned.1.call-start = ((), (), s32[]{:S(2)}) async-start(), calls=%async_computation.10 | async-start | bytes 442368 | tf_op jit(solution)/shard_map/reduce_scatter | solution.py:59
  21.6 316.6 %reduce-scatter.16.cloned.1.call-start = ((), (), s32[]{:S(2)}) async-start(), calls=%async_computation.11 | async-start | bytes 442368 | tf_op jit(solution)/shard_map/reduce_scatter | solution.py:62
  22.7 388.7 %reduce-scatter.18.cloned.1.call-start = ((), (), s32[]{:S(2)}) async-start(), calls=%async_computation.12 | async-start | bytes 327680 | tf_op jit(solution)/shard_map/reduce_scatter | solution.py:100
  352.1 2.7 copy-start.1
  354.8 5.5 copy-start.9
  354.8 36.4 %copy-start.4 = (bf16[768,512]{1,0:T(8,128)(2,1)S(1)}, bf16[768,512]{1,0:T(8,128)(2,1)}, u32[]{:S(2)}) copy-start(bf16[768,512]{1,0:T(8,128)(2,1)} %param.26) | copy-start | bytes 2359300
  354.8 56.6 %copy-start.6 = (bf16[128,128]{1,0:T(8,128)(2,1)S(1)}, bf16[128,128]{1,0:T(8,128)(2,1)}, u32[]{:S(2)}) copy-start(bf16[128,128]{1,0:T(8,128)(2,1)} %param.15) | copy-start | bytes 98308
  392.1 76.4 %all-gather.3.cloned.1.call-start = ((), (), s32[]{:S(2)}) async-start(), calls=%async_computation.14 | async-start | bytes 1081344 | tf_op jit(solution)/shard_map/all_gather | solution.py:102
  412.9 207.7 %reduce-scatter.20.cloned.1.call-start = ((), (), s32[]{:S(2)}) async-start(), calls=%async_computation.13 | async-start | bytes 2162688 | tf_op jit(solution)/shard_map/reduce_scatter | solution.py:105
  468.5 6.3 %copy-start.8 = (f32[4096]{0:T(1024)S(1)}, f32[4096]{0:T(1024)}, u32[]{:S(2)}) copy-start(f32[4096]{0:T(1024)} %param.27) | copy-start | bytes 49156
  476.5 144.2 %copy-start.5 = (bf16[128,128]{1,0:T(8,128)(2,1)S(1)}, bf16[128,128]{1,0:T(8,128)(2,1)}, u32[]{:S(2)}) copy-start(bf16[128,128]{1,0:T(8,128)(2,1)} %add_convert_fusion.1) | copy-start | bytes 98308
Sparse Core Ops, SparseCore 0:
  15.9 64.0 reduce-scatter.7
  83.2 61.1 reduce-scatter.9
  147.7 61.1 reduce-scatter.11
  212.1 61.1 reduce-scatter.13
  277.0 61.2 reduce-scatter.15
  392.2 19.1 reduce-scatter.17
  414.9 53.6 all-gather.2
  483.2 137.4 reduce-scatter.19
